TPU v7x, 32 devices: a whole 2x2x4 slice. The times are simulated.
32 devices in a mesh: grp: 2 (over y), sp: 4 (over z), tp: 4 (over x, core).
Axes of the slice: x: 2, y: 2, z: 4, core: 2. Of those that a mesh axis runs over, the one named last changes fastest.
Arguments:
- tokens_in: bfloat16 [2048, 2048], P(('grp', 'sp'), 'tp'), parts along dimension 0, may hold values from -6 to 6
- norm_gain: float32 [3, 2048], replicated, may hold values from 0.1 to 1.9
- w_pool_in: bfloat16 [3, 2048, 1024], P(None, 'sp', 'tp'), may hold values from -0.125 to 0.125
- w_gate: bfloat16 [3, 2048, 2048], P(None, 'sp', 'tp'), may hold values from -0.125 to 0.125
- w_back: bfloat16 [3, 1024, 2048], P(None, 'tp', 'sp'), may hold values from -0.25 to 0.25
Outputs:
- tokens_out: bfloat16 [2048, 2048], P(('grp', 'sp'), 'tp'), parts along dimension 0
There are 2 independent parts, one for each index of `grp`. A program takes and returns all parts, laid end to end along the dimension named above; an argument that names none is the same for every part. Nothing has to cross between parts.
All inputs are finite; a program needn't handle non-finite values.
Results may differ from a plain program's by a relative error of at most 0.017.
Values may be sent and summed in bfloat16 or wider, within the bound.
A program may use at most 64 MiB of HBM per device.

v0:
```python
import jax
import jax.numpy as jnp
from jax import lax
from jax.sharding import PartitionSpec as P

POOL_WIDTH = 1024
GROUPS = 4
GRID_W = 32
LAYERS = 3
pool_windows = (2, 4, 8, 16)
norm_eps = 1e-06


def padded_2(value, sides, width):
    for axis, dim in sides:
        peers, length = (lax.axis_size(axis), value.shape[dim])
        up = [(i, (i + 1) % peers) for i in range(peers - 1)]
        down = [(j, i) for i, j in up]
        last = lax.slice_in_dim(value, length - width, length, axis=dim)
        initial = lax.slice_in_dim(value, 0, width, axis=dim)
        before = lax.ppermute(last, axis, up)
        after = lax.ppermute(initial, axis, down)
        value = jnp.concatenate([before, value, after], axis=dim)
    return value


def window_means(padded, rows_here, first_row, total_rows, window):
    reach = max(pool_windows) // 2
    half_span = window // 2
    width_cols = padded.shape[1] - 2 * reach
    row_sums = padded[reach - half_span : reach - half_span + rows_here]
    for offset in range(1 - half_span, half_span):
        row_sums = row_sums + padded[reach + offset : reach + offset + rows_here]
    box_sums = row_sums[:, reach - half_span : reach - half_span + width_cols]
    for offset in range(1 - half_span, half_span):
        box_sums = box_sums + row_sums[:, reach + offset : reach + offset + width_cols]
    row_index = first_row + jnp.arange(rows_here, dtype=jnp.int32)
    col_index = jnp.arange(width_cols, dtype=jnp.int32)
    row_counts = jnp.minimum(row_index + half_span, total_rows) - jnp.maximum(
        row_index - half_span, 0
    )
    col_counts = jnp.minimum(col_index + half_span, width_cols) - jnp.maximum(
        col_index - half_span, 0
    )
    counts = (row_counts[:, None] * col_counts[None, :]).astype(jnp.float32)
    return box_sums / counts[:, :, None]


def on_device(tokens_in, norm_gain, w_pool_in, w_gate, w_back):
    reach = max(pool_windows) // 2
    sp_count = lax.axis_size("sp")
    tp_count = lax.axis_size("tp")
    tp_pos = lax.axis_index("tp")
    sp_pos = lax.axis_index("sp")
    tok_rows = tokens_in.shape[0]
    rows_here = tok_rows // GRID_W
    total_rows = rows_here * sp_count
    first_row = sp_pos * rows_here
    local_pool = w_pool_in.shape[2]
    group_width = POOL_WIDTH // GROUPS
    channel_group = (tp_pos * local_pool + jnp.arange(local_pool, dtype=jnp.int32)) // group_width
    state = tokens_in
    for layer_id in range(LAYERS):
        whole_rows = lax.all_gather(state, "tp", axis=1, tiled=True)
        wide = whole_rows.astype(jnp.float32)
        normed = (
            wide
            * lax.rsqrt(jnp.mean(wide * wide, axis=-1, keepdims=True) + norm_eps)
            * norm_gain[layer_id]
        ).astype(jnp.bfloat16)
        pool_acc = jnp.dot(
            normed,
            lax.all_gather(w_pool_in[layer_id], "sp", axis=0, tiled=True),
            preferred_element_type=jnp.float32,
        )
        gate_acc = jnp.dot(
            normed,
            lax.all_gather(w_gate[layer_id], "sp", axis=0, tiled=True),
            preferred_element_type=jnp.float32,
        )
        pool_in = pool_acc.astype(jnp.bfloat16)
        gate = jax.nn.sigmoid(gate_acc)
        cells = pool_in.reshape(rows_here, GRID_W, local_pool)
        rimmed = padded_2(cells, (("sp", 0),), reach)
        padded = jnp.pad(rimmed.astype(jnp.float32), ((0, 0), (reach, reach), (0, 0)))
        means = jnp.zeros((rows_here, GRID_W, local_pool), jnp.float32)
        for group_id in range(GROUPS):
            in_group = (channel_group == group_id)[None, None, :]
            means = jnp.where(
                in_group,
                window_means(padded, rows_here, first_row, total_rows, pool_windows[group_id]),
                means,
            )
        pooled = (
            (means - cells.astype(jnp.float32)).reshape(tok_rows, local_pool).astype(jnp.bfloat16)
        )
        full_pooled = lax.all_gather(pooled, "tp", axis=1, tiled=True)
        back_rows = lax.all_gather(w_back[layer_id], "sp", axis=1, tiled=True)
        back_cols = lax.all_to_all(back_rows, "tp", split_axis=1, concat_axis=0, tiled=True)
        partials = jnp.einsum(
            "tnb,nbd->ntd",
            full_pooled.reshape(tok_rows, tp_count, local_pool),
            back_cols.reshape(tp_count, local_pool, back_cols.shape[1]),
            preferred_element_type=jnp.float32,
        ).astype(jnp.bfloat16)
        branch = jnp.sum(partials.astype(jnp.float32), axis=0)
        state = (state.astype(jnp.float32) + gate * branch).astype(jnp.bfloat16)
    return state


def solution(mesh):
    return jax.shard_map(
        on_device,
        mesh=mesh,
        in_specs=(
            P(("grp", "sp"), "tp"),
            P(),
            P(None, "sp", "tp"),
            P(None, "sp", "tp"),
            P(None, "tp", "sp"),
        ),
        out_specs=P(("grp", "sp"), "tp"),
        check_vma=False,
    )
```

profile of v0, /device:TPU:0, one launch (start us, length us, event | category | flops | bytes accessed | tf_op | source)
XLA Modules:
  0.0 391.0 jit_solution(7945444731493379469)
XLA Ops:
  7.3 2.2 fusion.168
  13.5 14.9 %all-gather.22.cloned.1.call-done = bf16[256,2048]{1,0:T(8,128)(2,1)} async-done(((bf16[256,512]{1,0:T(8,128)(2,1)}), bf16[256,2048]{1,0:T(8,128)(2,1)}) %all-gather.22.cloned.1.call-update) | async-done | bytes 1048592 | tf_op jit(solution)/shard_map/all_gather | solution.py:64
  29.9 28.1 %all-gather.30.cloned.1.call-done = bf16[1,2048,256]{2,1,0:T(8,128)(2,1)} async-done(((bf16[1,512,256]{2,1,0:T(8,128)(2,1)}), bf16[1,2048,256]{2,1,0:T(8,128)(2,1)}) %all-gather.30.cloned.1.call-update) | async-done | bytes 1048592 | tf_op jit(solution)/shard_map/all_gather | solution.py:73
  57.9 2.0 convolution_convert_fusion.5
  60.0 3.4 collective-permute-start
  64.7 23.0 %all-gather.32.cloned.1.call-done = bf16[1,256,2048]{1,2,0:T(8,128)(2,1)} async-done(((bf16[1,256,512]{1,2,0:T(8,128)(2,1)}), bf16[1,256,2048]{1,2,0:T(8,128)(2,1)}) %all-gather.32.cloned.1.call-update) | async-done | bytes 1048592 | tf_op jit(solution)/shard_map/all_gather | solution.py:98
  87.7 2.3 copy.20
  90.0 3.5 all-to-all-start
  94.9 16.6 %all_gather.48 = bf16[256,1024]{1,0:T(8,128)(2,1)S(1)} all-gather(bf16[256,256]{1,0:T(8,128)(2,1)S(1)} %bitcast.112), channel_id=1, replica_groups=mesh['grp'=2,'sp'=4,'tp'=4] {'tp'}, dimensions={1}, use_global_device_ids=true | all-gather | bytes 655360 | tf_op jit(solution)/shard_map/all_gather | solution.py:97
  112.3 21.1 %all-gather.28.cloned.1.call-done = bf16[1,2048,512]{2,1,0:T(8,128)(2,1)} async-done(((bf16[1,512,512]{2,1,0:T(8,128)(2,1)}), bf16[1,2048,512]{2,1,0:T(8,128)(2,1)}) %all-gather.28.cloned.1.call-update) | async-done | bytes 2097168 | tf_op jit(solution)/shard_map/all_gather | solution.py:78
  133.4 3.2 fusion.75
  138.8 13.4 %all-gather.24.cloned.1.call-done = bf16[256,2048]{1,0:T(8,128)(2,1)} async-done(((bf16[256,512]{1,0:T(8,128)(2,1)}), bf16[256,2048]{1,0:T(8,128)(2,1)}) %all-gather.24.cloned.1.call-update) | async-done | bytes 1048592 | tf_op jit(solution)/shard_map/all_gather | solution.py:64
  152.2 1.5 fusion.3
  153.8 27.9 %all-gather.36.cloned.1.call-done = bf16[1,2048,256]{2,1,0:T(8,128)(2,1)} async-done(((bf16[1,512,256]{2,1,0:T(8,128)(2,1)}), bf16[1,2048,256]{2,1,0:T(8,128)(2,1)}) %all-gather.36.cloned.1.call-update) | async-done | bytes 1048592 | tf_op jit(solution)/shard_map/all_gather | solution.py:73
  181.7 2.0 convolution_convert_fusion.4
  183.7 3.4 collective-permute-start.2
  188.4 23.1 %all-gather.38.cloned.1.call-done = bf16[1,256,2048]{1,2,0:T(8,128)(2,1)} async-done(((bf16[1,256,512]{1,2,0:T(8,128)(2,1)}), bf16[1,256,2048]{1,2,0:T(8,128)(2,1)}) %all-gather.38.cloned.1.call-update) | async-done | bytes 1048592 | tf_op jit(solution)/shard_map/all_gather | solution.py:98
  211.5 2.3 copy.24
  213.7 3.5 all-to-all-start.1
  219.2 16.1 %all_gather.53 = bf16[256,1024]{1,0:T(8,128)(2,1)S(1)} all-gather(bf16[256,256]{1,0:T(8,128)(2,1)S(1)} %bitcast.113), channel_id=1, replica_groups=mesh['grp'=2,'sp'=4,'tp'=4] {'tp'}, dimensions={1}, use_global_device_ids=true | all-gather | bytes 655360 | tf_op jit(solution)/shard_map/all_gather | solution.py:97
  236.0 21.2 %all-gather.34.cloned.1.call-done = bf16[1,2048,512]{2,1,0:T(8,128)(2,1)} async-done(((bf16[1,512,512]{2,1,0:T(8,128)(2,1)}), bf16[1,2048,512]{2,1,0:T(8,128)(2,1)}) %all-gather.34.cloned.1.call-update) | async-done | bytes 2097168 | tf_op jit(solution)/shard_map/all_gather | solution.py:78
  257.3 3.1 fusion.72
  262.5 13.6 %all-gather.26.cloned.1.call-done = bf16[256,2048]{1,0:T(8,128)(2,1)} async-done(((bf16[256,512]{1,0:T(8,128)(2,1)}), bf16[256,2048]{1,0:T(8,128)(2,1)}) %all-gather.26.cloned.1.call-update) | async-done | bytes 1048592 | tf_op jit(solution)/shard_map/all_gather | solution.py:64
  277.6 27.9 %all-gather.42.cloned.1.call-done = bf16[1,2048,256]{2,1,0:T(8,128)(2,1)} async-done(((bf16[1,512,256]{2,1,0:T(8,128)(2,1)}), bf16[1,2048,256]{2,1,0:T(8,128)(2,1)}) %all-gather.42.cloned.1.call-update) | async-done | bytes 1048592 | tf_op jit(solution)/shard_map/all_gather | solution.py:73
  305.5 2.0 convolution_convert_fusion.3
  307.6 3.4 collective-permute-start.4
  312.2 23.1 %all-gather.44.cloned.1.call-done = bf16[1,256,2048]{1,2,0:T(8,128)(2,1)} async-done(((bf16[1,256,512]{1,2,0:T(8,128)(2,1)}), bf16[1,256,2048]{1,2,0:T(8,128)(2,1)}) %all-gather.44.cloned.1.call-update) | async-done | bytes 1048592 | tf_op jit(solution)/shard_map/all_gather | solution.py:98
  335.3 2.3 copy.28
  337.6 3.7 all-to-all-start.2
  343.1 16.1 %all_gather.58 = bf16[256,1024]{1,0:T(8,128)(2,1)S(1)} all-gather(bf16[256,256]{1,0:T(8,128)(2,1)S(1)} %bitcast.111), channel_id=1, replica_groups=mesh['grp'=2,'sp'=4,'tp'=4] {'tp'}, dimensions={1}, use_global_device_ids=true | all-gather | bytes 655360 | tf_op jit(solution)/shard_map/all_gather | solution.py:97
  359.9 21.1 %all-gather.40.cloned.1.call-done = bf16[1,2048,512]{2,1,0:T(8,128)(2,1)} async-done(((bf16[1,512,512]{2,1,0:T(8,128)(2,1)}), bf16[1,2048,512]{2,1,0:T(8,128)(2,1)}) %all-gather.40.cloned.1.call-update) | async-done | bytes 2097168 | tf_op jit(solution)/shard_map/all_gather | solution.py:78
  381.0 3.1 fusion.69
  (129 shorter events, 22.9 us)
Async XLA Ops:
  6.5 21.8 %all-gather.22.cloned.1.call-start = ((), (), s32[]{:S(2)}) async-start(), calls=%async_computation.3 | async-start | bytes 1310720 | tf_op jit(solution)/shard_map/all_gather | solution.py:64
  7.3 50.7 %all-gather.30.cloned.1.call-start = ((), (), s32[]{:S(2)}) async-start(), calls=%async_computation.7 | async-start | bytes 1310720 | tf_op jit(solution)/shard_map/all_gather | solution.py:73
  9.5 78.2 %all-gather.32.cloned.1.call-start = ((), (), s32[]{:S(2)}) async-start(), calls=%async_computation.8 | async-start | bytes 1310720 | tf_op jit(solution)/shard_map/all_gather | solution.py:98
  11.2 122.2 %all-gather.28.cloned.1.call-start = ((), (), s32[]{:S(2)}) async-start(), calls=%async_computation.6 | async-start | bytes 2621440 | tf_op jit(solution)/shard_map/all_gather | solution.py:78
  13.5 46.5 %copy-start.10 = (f32[1,2048]{1,0:T(1,128)}, f32[1,2048]{1,0:T(1,128)S(1)}, u32[]{:S(2)}) copy-start(f32[1,2048]{1,0:T(1,128)S(1)} %get-tuple-element.27) | copy-start | bytes 24580
  29.9 60.1 %copy-start.23 = (f32[256]{0:T(256)}, f32[256]{0:T(256)S(1)}, u32[]{:S(2)}) copy-start(f32[256]{0:T(256)S(1)} %add_rsqrt_fusion.2) | copy-start | bytes 3076
  60.0 33.6 %collective-permute-start = (bf16[8,32,256]{2,1,0:T(8,128)(2,1)S(1)}, bf16[8,32,256]{2,1,0:T(8,128)(2,1)S(1)}, u32[]{:S(2)}, u32[]{:S(2)}) collective-permute-start(bf16[8,32,256]{2,1,0:T(8,128)(2,1)S(1)} %bitcast.99), channel_id=1, source_target_pairs={{0,4},{4,8},{8,12},{1,5},{5,9},{9,13},{2,6},{6,10},{10,14},{3,7},{... | collective-permute-start | bytes 393224 | tf_op jit(solution)/shard_map/ppermute | solution.py:21
  63.3 30.2 %collective-permute-start.1 = (bf16[8,32,256]{2,1,0:T(8,128)(2,1)S(1)}, bf16[8,32,256]{2,1,0:T(8,128)(2,1)S(1)}, u32[]{:S(2)}, u32[]{:S(2)}) collective-permute-start(bf16[8,32,256]{2,1,0:T(8,128)(2,1)S(1)} %bitcast.100), channel_id=1, source_target_pairs={{4,0},{8,4},{12,8},{5,1},{9,5},{13,9},{6,2},{10,6},{14,10},{7,3},{... | collective-permute-start | bytes 393224 | tf_op jit(solution)/shard_map/ppermute | solution.py:22
  64.7 29.4 %copy-start.11 = (pred[256]{0:T(512)(128)(4,1)}, pred[256]{0:T(512)(128)(4,1)S(1)}, u32[]{:S(2)}) copy-start(pred[256]{0:T(512)(128)(4,1)S(1)} %get-tuple-element.33) | copy-start | bytes 772
  90.0 21.8 %all-to-all-start = ((bf16[256,4,512]{2,0,1:T(8,128)(2,1)}), bf16[256,4,512]{2,0,1:T(8,128)(2,1)S(1)}, u32[]{:S(2)}, u32[]{:S(2)}) async-start(bf16[256,4,512]{2,0,1:T(8,128)(2,1)} %copy.20), calls=%async_computation | async-start | bytes 2097152 | tf_op jit(solution)/shard_map/all_to_all | solution.py:99
  93.5 58.7 %all-gather.24.cloned.1.call-start = ((), (), s32[]{:S(2)}) async-start(), calls=%async_computation.4 | async-start | bytes 1310720 | tf_op jit(solution)/shard_map/all_gather | solution.py:64
  94.9 38.5 %copy-start.1 = (bf16[256,2048]{1,0:T(8,128)(2,1)S(1)}, bf16[256,2048]{1,0:T(8,128)(2,1)}, u32[]{:S(2)}) copy-start(bf16[256,2048]{1,0:T(8,128)(2,1)} %all-gather.22.cloned.1.call-done) | copy-start | bytes 3145732
  136.5 45.1 %copy-start.8 = (f32[1,2048]{1,0:T(1,128)S(1)}, f32[1,2048]{1,0:T(1,128)}, u32[]{:S(2)}) copy-start(f32[1,2048]{1,0:T(1,128)} %get-tuple-element.28) | copy-start | bytes 24580
  136.6 45.1 %all-gather.36.cloned.1.call-start = ((), (), s32[]{:S(2)}) async-start(), calls=%async_computation.10 | async-start | bytes 1310720 | tf_op jit(solution)/shard_map/all_gather | solution.py:73
  137.1 74.3 %all-gather.38.cloned.1.call-start = ((), (), s32[]{:S(2)}) async-start(), calls=%async_computation.11 | async-start | bytes 1310720 | tf_op jit(solution)/shard_map/all_gather | solution.py:98
  138.1 119.2 %all-gather.34.cloned.1.call-start = ((), (), s32[]{:S(2)}) async-start(), calls=%async_computation.9 | async-start | bytes 2621440 | tf_op jit(solution)/shard_map/all_gather | solution.py:78
  153.8 60.0 %copy-start.24 = (f32[256]{0:T(256)}, f32[256]{0:T(256)S(1)}, u32[]{:S(2)}) copy-start(f32[256]{0:T(256)S(1)} %add_rsqrt_fusion.1) | copy-start | bytes 3076
  183.7 33.6 %collective-permute-start.2 = (bf16[8,32,256]{2,1,0:T(8,128)(2,1)S(1)}, bf16[8,32,256]{2,1,0:T(8,128)(2,1)S(1)}, u32[]{:S(2)}, u32[]{:S(2)}) collective-permute-start(bf16[8,32,256]{2,1,0:T(8,128)(2,1)S(1)} %bitcast.107), channel_id=1, source_target_pairs={{0,4},{4,8},{8,12},{1,5},{5,9},{9,13},{2,6},{6,10},{10,14},{3,7},{... | collective-permute-start | bytes 393224 | tf_op jit(solution)/shard_map/ppermute | solution.py:21
  187.1 30.3 %collective-permute-start.3 = (bf16[8,32,256]{2,1,0:T(8,128)(2,1)S(1)}, bf16[8,32,256]{2,1,0:T(8,128)(2,1)S(1)}, u32[]{:S(2)}, u32[]{:S(2)}) collective-permute-start(bf16[8,32,256]{2,1,0:T(8,128)(2,1)S(1)} %bitcast.108), channel_id=1, source_target_pairs={{4,0},{8,4},{12,8},{5,1},{9,5},{13,9},{6,2},{10,6},{14,10},{7,3},{... | collective-permute-start | bytes 393224 | tf_op jit(solution)/shard_map/ppermute | solution.py:22
  213.7 21.8 %all-to-all-start.1 = ((bf16[256,4,512]{2,0,1:T(8,128)(2,1)}), bf16[256,4,512]{2,0,1:T(8,128)(2,1)S(1)}, u32[]{:S(2)}, u32[]{:S(2)}) async-start(bf16[256,4,512]{2,0,1:T(8,128)(2,1)} %copy.24), calls=%async_computation.1 | async-start | bytes 2097152 | tf_op jit(solution)/shard_map/all_to_all | solution.py:99
  217.3 58.8 %all-gather.26.cloned.1.call-start = ((), (), s32[]{:S(2)}) async-start(), calls=%async_computation.5 | async-start | bytes 1310720 | tf_op jit(solution)/shard_map/all_gather | solution.py:64
  219.2 38.1 %copy-start.3 = (bf16[256,2048]{1,0:T(8,128)(2,1)S(1)}, bf16[256,2048]{1,0:T(8,128)(2,1)}, u32[]{:S(2)}) copy-start(bf16[256,2048]{1,0:T(8,128)(2,1)} %all-gather.24.cloned.1.call-done) | copy-start | bytes 3145732
  219.2 38.0 %copy-start.9 = (f32[1,2048]{1,0:T(1,128)S(1)}, f32[1,2048]{1,0:T(1,128)}, u32[]{:S(2)}) copy-start(f32[1,2048]{1,0:T(1,128)} %get-tuple-element.28) | copy-start | bytes 24580
  219.2 38.0 %copy-start.25 = (f32[256]{0:T(256)S(1)}, f32[256]{0:T(256)}, u32[]{:S(2)}) copy-start(f32[256]{0:T(256)} %copy-done.24) | copy-start | bytes 3076
  260.4 45.1 %copy-start.7 = (f32[1,2048]{1,0:T(1,128)S(1)}, f32[1,2048]{1,0:T(1,128)}, u32[]{:S(2)}) copy-start(f32[1,2048]{1,0:T(1,128)} %get-tuple-element.26) | copy-start | bytes 24580
  260.4 45.1 %all-gather.42.cloned.1.call-start = ((), (), s32[]{:S(2)}) async-start(), calls=%async_computation.13 | async-start | bytes 1310720 | tf_op jit(solution)/shard_map/all_gather | solution.py:73
  261.0 74.3 %all-gather.44.cloned.1.call-start = ((), (), s32[]{:S(2)}) async-start(), calls=%async_computation.14 | async-start | bytes 1310720 | tf_op jit(solution)/shard_map/all_gather | solution.py:98
  261.9 119.0 %all-gather.40.cloned.1.call-start = ((), (), s32[]{:S(2)}) async-start(), calls=%async_computation.12 | async-start | bytes 2621440 | tf_op jit(solution)/shard_map/all_gather | solution.py:78
  307.6 33.7 %collective-permute-start.4 = (bf16[8,32,256]{2,1,0:T(8,128)(2,1)S(1)}, bf16[8,32,256]{2,1,0:T(8,128)(2,1)S(1)}, u32[]{:S(2)}, u32[]{:S(2)}) collective-permute-start(bf16[8,32,256]{2,1,0:T(8,128)(2,1)S(1)} %bitcast.103), channel_id=1, source_target_pairs={{0,4},{4,8},{8,12},{1,5},{5,9},{9,13},{2,6},{6,10},{10,14},{3,7},{... | collective-permute-start | bytes 393224 | tf_op jit(solution)/shard_map/ppermute | solution.py:21
  310.9 30.4 %collective-permute-start.5 = (bf16[8,32,256]{2,1,0:T(8,128)(2,1)S(1)}, bf16[8,32,256]{2,1,0:T(8,128)(2,1)S(1)}, u32[]{:S(2)}, u32[]{:S(2)}) collective-permute-start(bf16[8,32,256]{2,1,0:T(8,128)(2,1)S(1)} %bitcast.104), channel_id=1, source_target_pairs={{4,0},{8,4},{12,8},{5,1},{9,5},{13,9},{6,2},{10,6},{14,10},{7,3},{... | collective-permute-start | bytes 393224 | tf_op jit(solution)/shard_map/ppermute | solution.py:22
  337.6 21.8 %all-to-all-start.2 = ((bf16[256,4,512]{2,0,1:T(8,128)(2,1)}), bf16[256,4,512]{2,0,1:T(8,128)(2,1)S(1)}, u32[]{:S(2)}, u32[]{:S(2)}) async-start(bf16[256,4,512]{2,0,1:T(8,128)(2,1)} %copy.28), calls=%async_computation.2 | async-start | bytes 2097152 | tf_op jit(solution)/shard_map/all_to_all | solution.py:99
  343.1 37.9 %copy-start.2 = (bf16[256,2048]{1,0:T(8,128)(2,1)S(1)}, bf16[256,2048]{1,0:T(8,128)(2,1)}, u32[]{:S(2)}) copy-start(bf16[256,2048]{1,0:T(8,128)(2,1)} %all-gather.26.cloned.1.call-done) | copy-start | bytes 3145732
  (15 other events, 127.0 us)
Sparse Core Ops, SparseCore 0:
  8.9 19.4 all-gather.21
  29.9 27.9 all-gather.29
  59.5 28.1 all-gather.31
  89.1 44.1 all-gather.27
  136.7 15.4 all-gather.23
  153.7 27.9 all-gather.35
  183.2 28.1 all-gather.37
  213.0 44.1 all-gather.33
  260.6 15.4 all-gather.25
  277.5 27.9 all-gather.41
  307.1 28.1 all-gather.43
  336.7 44.2 all-gather.39
where the time goes:
time: 392 us; the launch traced here: 391 us
  waiting for transfers between devices  261 us (67%)
  blocking collectives  48.8 us (12%)
  starting transfers between devices  25.1 us (6%)
  matrix products  16.9 us (4%)
  local copies, waits for them, and re-layouts  15.8 us (4%)
  between operations  14.2 us (4%)
  other arithmetic  8.76 us (2%)
    all_gather x3, waiting for transfers between devices, on_device(): lax.all_gather(w_pool_in[layer_id], 'sp', axis=0, tiled=True)  83.9 us
    all_gather x3, waiting for transfers between devices, on_device(): back_rows = lax.all_gather(w_back[layer_id], 'sp', axis=1, tiled=True)  69.2 us
    all_gather x3, waiting for transfers between devices, on_device(): lax.all_gather(w_gate[layer_id], 'sp', axis=0, tiled=True)  63.4 us
    all_gather x3, blocking collectives, on_device(): full_pooled = lax.all_gather(pooled, 'tp', axis=1, tiled=True)  48.8 us
    all_gather x3, waiting for transfers between devices, on_device(): whole_rows = lax.all_gather(state, 'tp', axis=1, tiled=True)  41.8 us
    all_to_all x3, starting transfers between devices, on_device(): lax.all_to_all(back_rows, 'tp', split_axis=1, concat_axis=0, tiled=True)  10.7 us
    ppermute x3, starting transfers between devices, padded_2(): before = lax.ppermute(last, axis, up)  10.1 us
    dot_general x3, matrix products, on_device(): jnp.dot(normed, lax.all_gather(w_gate[layer_id], 'sp', axis=0, tiled=True...  9.41 us
  transfers between devices with their start and end apart: 21, of which 12 were waited for; matrix products, arithmetic and copies ran while one was open for 8% of the time, Pallas kernels for 0%

commit v1 on v0

--- a/solution.py
+++ b/solution.py
@@ -2,6 +2,7 @@
 import jax.numpy as jnp
 from jax import lax
 from jax.sharding import PartitionSpec as P
+from jax.lax import axis_index, ppermute, psum
 
 POOL_WIDTH = 1024
 GROUPS = 4
@@ -61,7 +62,21 @@
     channel_group = (tp_pos * local_pool + jnp.arange(local_pool, dtype=jnp.int32)) // group_width
     state = tokens_in
     for layer_id in range(LAYERS):
-        whole_rows = lax.all_gather(state, "tp", axis=1, tiled=True)
+
+        def trace_case(sample, mesh_dim, which_dim=1):
+            full_n = psum(1, mesh_dim)
+            view_out = sample
+            seen = [view_out]
+            outer = sorted(((kk, (kk + 1) % full_n) for kk in range(full_n)))
+            for dev_i in range(1, full_n):
+                view_out = ppermute(view_out, mesh_dim, outer)
+                seen.insert(0, view_out)
+            arr_now = jnp.concatenate(seen, which_dim)
+            small = axis_index(mesh_dim) + 1
+            h_now = jnp.roll(arr_now, small * sample.shape[which_dim], which_dim)
+            return h_now
+
+        whole_rows = trace_case(state, "tp")
         wide = whole_rows.astype(jnp.float32)
         normed = (
             wide

time: 392 us -> 333 us (0.85)
  waiting for transfers between devices: 261 us -> 202 us
  other arithmetic: 8.76 us -> 12.8 us
    all_gather x3, waiting for transfers between devices: 83.9 us -> 17.2 us  [on_device(): lax.all_gather(w_pool_in[layer_id], 'sp', axis=0, tiled=True)]
    ppermute x0 -> x9, waiting for transfers between devices: none -> 51.2 us  [trace_case(): view_out = ppermute(view_out, mesh_dim, outer)]
    all_gather x3 -> x0, waiting for transfers between devices: 41.8 us -> none  [on_device(): whole_rows = lax.all_gather(state, 'tp', axis=1, tiled=True)]
    reduce_sum x3, other arithmetic: 4.53 us -> 8.56 us  [on_device(): jnp.mean(wide * wide, axis=-1, keepdims=True) + norm_eps]
  transfers between devices with their start and end apart: 21 -> 27, of which waited for: 12 -> 18; matrix products, arithmetic and copies ran while one was open for 8% -> 11% of each run, Pallas kernels for 0% -> 0%
where the time goes in v1:
time: 333 us; the launch traced here: 332 us
  waiting for transfers between devices  202 us (61%)
  blocking collectives  48.7 us (15%)
  starting transfers between devices  25.7 us (8%)
  local copies, waits for them, and re-layouts  15.1 us (5%)
  matrix products  14.6 us (4%)
  between operations  13.8 us (4%)
  other arithmetic  12.8 us (4%)
    all_gather x3, waiting for transfers between devices, on_device(): back_rows = lax.all_gather(w_back[layer_id], 'sp', axis=1, tiled=True)  67.5 us
    all_gather x3, waiting for transfers between devices, on_device(): lax.all_gather(w_gate[layer_id], 'sp', axis=0, tiled=True)  65.1 us
    ppermute x9, waiting for transfers between devices, trace_case(): view_out = ppermute(view_out, mesh_dim, outer)  51.2 us
    all_gather x3, blocking collectives, on_device(): full_pooled = lax.all_gather(pooled, 'tp', axis=1, tiled=True)  48.7 us
    all_gather x3, waiting for transfers between devices, on_device(): lax.all_gather(w_pool_in[layer_id], 'sp', axis=0, tiled=True)  17.2 us
    all_to_all x3, starting transfers between devices, on_device(): lax.all_to_all(back_rows, 'tp', split_axis=1, concat_axis=0, tiled=True)  10.8 us
    ppermute x3, starting transfers between devices, padded_2(): before = lax.ppermute(last, axis, up)  10.1 us
    reduce_sum x3, other arithmetic, on_device(): jnp.mean(wide * wide, axis=-1, keepdims=True) + norm_eps  8.56 us
  transfers between devices with their start and end apart: 27, of which 18 were waited for; matrix products, arithmetic and copies ran while one was open for 11% of the time, Pallas kernels for 0%

profile of v1, /device:TPU:0, one launch (start us, length us, event | category | flops | bytes accessed | tf_op | source)
XLA Modules:
  0.0 332.4 jit_solution(5592557218177108179)
XLA Ops:
  13.8 5.2 %collective-permute-done = bf16[256,512]{1,0:T(8,128)(2,1)S(1)} collective-permute-done((bf16[256,512]{1,0:T(8,128)(2,1)S(1)}, bf16[256,512]{1,0:T(8,128)(2,1)S(1)}, u32[]{:S(2)}, u32[]{:S(2)}) %collective-permute-start) | collective-permute-done | bytes 262176 | tf_op jit(solution)/shard_map/ppermute | solution.py:72
  19.1 5.7 %collective-permute-done.1 = bf16[256,512]{1,0:T(8,128)(2,1)S(1)} collective-permute-done((bf16[256,512]{1,0:T(8,128)(2,1)S(1)}, bf16[256,512]{1,0:T(8,128)(2,1)S(1)}, u32[]{:S(2)}, u32[]{:S(2)}) %collective-permute-start.1) | collective-permute-done | bytes 262176 | tf_op jit(solution)/shard_map/ppermute | solution.py:72
  25.0 5.7 %collective-permute-done.2 = bf16[256,512]{1,0:T(8,128)(2,1)S(1)} collective-permute-done((bf16[256,512]{1,0:T(8,128)(2,1)S(1)}, bf16[256,512]{1,0:T(8,128)(2,1)S(1)}, u32[]{:S(2)}, u32[]{:S(2)}) %collective-permute-start.2) | collective-permute-done | bytes 262176 | tf_op jit(solution)/shard_map/ppermute | solution.py:72
  30.6 2.8 fusion
  33.5 6.1 %all-gather.21.cloned.1.call-done = bf16[1,2048,256]{2,1,0:T(8,128)(2,1)} async-done(((bf16[1,512,256]{2,1,0:T(8,128)(2,1)}), bf16[1,2048,256]{2,1,0:T(8,128)(2,1)}) %all-gather.21.cloned.1.call-update) | async-done | bytes 1048592 | tf_op jit(solution)/shard_map/all_gather | solution.py:88
  41.4 3.4 %collective-permute-start.3 = (bf16[8,32,256]{2,1,0:T(8,128)(2,1)S(1)}, bf16[8,32,256]{2,1,0:T(8,128)(2,1)S(1)}, u32[]{:S(2)}, u32[]{:S(2)}) collective-permute-start(bf16[8,32,256]{2,1,0:T(8,128)(2,1)S(1)} %bitcast.103), channel_id=1, source_target_pairs={{0,4},{4,8},{8,12},{1,5},{5,9},{9,13},{2,6},{6,10},{10,14},{3,7},{... | collective-permute-start | bytes 393224 | tf_op jit(solution)/shard_map/ppermute | solution.py:22
  46.1 22.7 %all-gather.23.cloned.1.call-done = bf16[1,256,2048]{1,2,0:T(8,128)(2,1)} async-done(((bf16[1,256,512]{1,2,0:T(8,128)(2,1)}), bf16[1,256,2048]{1,2,0:T(8,128)(2,1)}) %all-gather.23.cloned.1.call-update) | async-done | bytes 1048592 | tf_op jit(solution)/shard_map/all_gather | solution.py:113
  71.1 3.5 %all-to-all-start = ((bf16[256,4,512]{2,0,1:T(8,128)(2,1)}), bf16[256,4,512]{2,0,1:T(8,128)(2,1)S(1)}, u32[]{:S(2)}, u32[]{:S(2)}) async-start(bf16[256,4,512]{2,0,1:T(8,128)(2,1)} %copy.20), calls=%async_computation | async-start | bytes 2097152 | tf_op jit(solution)/shard_map/all_to_all | solution.py:114
  76.1 16.6 %all_gather.38 = bf16[256,1024]{1,0:T(8,128)(2,1)S(1)} all-gather(bf16[256,256]{1,0:T(8,128)(2,1)S(1)} %bitcast.112), channel_id=1, replica_groups=mesh['grp'=2,'sp'=4,'tp'=4] {'tp'}, dimensions={1}, use_global_device_ids=true | all-gather | bytes 655360 | tf_op jit(solution)/shard_map/all_gather | solution.py:112
  93.4 21.8 %all-gather.19.cloned.1.call-done = bf16[1,2048,512]{2,1,0:T(8,128)(2,1)} async-done(((bf16[1,512,512]{2,1,0:T(8,128)(2,1)}), bf16[1,2048,512]{2,1,0:T(8,128)(2,1)}) %all-gather.19.cloned.1.call-update) | async-done | bytes 2097168 | tf_op jit(solution)/shard_map/all_gather | solution.py:93
  115.2 2.4 fusion.75
  117.9 5.7 %collective-permute-done.5 = bf16[256,512]{1,0:T(8,128)(2,1)S(1)} collective-permute-done((bf16[256,512]{1,0:T(8,128)(2,1)S(1)}, bf16[256,512]{1,0:T(8,128)(2,1)S(1)}, u32[]{:S(2)}, u32[]{:S(2)}) %collective-permute-start.5) | collective-permute-done | bytes 262176 | tf_op jit(solution)/shard_map/ppermute | solution.py:72
  123.6 5.8 %collective-permute-done.6 = bf16[256,512]{1,0:T(8,128)(2,1)S(1)} collective-permute-done((bf16[256,512]{1,0:T(8,128)(2,1)S(1)}, bf16[256,512]{1,0:T(8,128)(2,1)S(1)}, u32[]{:S(2)}, u32[]{:S(2)}) %collective-permute-start.6) | collective-permute-done | bytes 262176 | tf_op jit(solution)/shard_map/ppermute | solution.py:72
  129.4 5.8 %collective-permute-done.7 = bf16[256,512]{1,0:T(8,128)(2,1)S(1)} collective-permute-done((bf16[256,512]{1,0:T(8,128)(2,1)S(1)}, bf16[256,512]{1,0:T(8,128)(2,1)S(1)}, u32[]{:S(2)}, u32[]{:S(2)}) %collective-permute-start.7) | collective-permute-done | bytes 262176 | tf_op jit(solution)/shard_map/ppermute | solution.py:72
  135.2 2.9 fusion.3
  138.0 5.4 %all-gather.27.cloned.1.call-done = bf16[1,2048,256]{2,1,0:T(8,128)(2,1)} async-done(((bf16[1,512,256]{2,1,0:T(8,128)(2,1)}), bf16[1,2048,256]{2,1,0:T(8,128)(2,1)}) %all-gather.27.cloned.1.call-update) | async-done | bytes 1048592 | tf_op jit(solution)/shard_map/all_gather | solution.py:88
  145.2 3.4 %collective-permute-start.8 = (bf16[8,32,256]{2,1,0:T(8,128)(2,1)S(1)}, bf16[8,32,256]{2,1,0:T(8,128)(2,1)S(1)}, u32[]{:S(2)}, u32[]{:S(2)}) collective-permute-start(bf16[8,32,256]{2,1,0:T(8,128)(2,1)S(1)} %bitcast.99), channel_id=1, source_target_pairs={{0,4},{4,8},{8,12},{1,5},{5,9},{9,13},{2,6},{6,10},{10,14},{3,7},{... | collective-permute-start | bytes 393224 | tf_op jit(solution)/shard_map/ppermute | solution.py:22
  150.7 22.1 %all-gather.29.cloned.1.call-done = bf16[1,256,2048]{1,2,0:T(8,128)(2,1)} async-done(((bf16[1,256,512]{1,2,0:T(8,128)(2,1)}), bf16[1,256,2048]{1,2,0:T(8,128)(2,1)}) %all-gather.29.cloned.1.call-update) | async-done | bytes 1048592 | tf_op jit(solution)/shard_map/all_gather | solution.py:113
  175.1 3.5 %all-to-all-start.1 = ((bf16[256,4,512]{2,0,1:T(8,128)(2,1)}), bf16[256,4,512]{2,0,1:T(8,128)(2,1)S(1)}, u32[]{:S(2)}, u32[]{:S(2)}) async-start(bf16[256,4,512]{2,0,1:T(8,128)(2,1)} %copy.24), calls=%async_computation.1 | async-start | bytes 2097152 | tf_op jit(solution)/shard_map/all_to_all | solution.py:114
  180.6 16.1 %all_gather.42 = bf16[256,1024]{1,0:T(8,128)(2,1)S(1)} all-gather(bf16[256,256]{1,0:T(8,128)(2,1)S(1)} %bitcast.113), channel_id=1, replica_groups=mesh['grp'=2,'sp'=4,'tp'=4] {'tp'}, dimensions={1}, use_global_device_ids=true | all-gather | bytes 655360 | tf_op jit(solution)/shard_map/all_gather | solution.py:112
  197.4 21.4 %all-gather.25.cloned.1.call-done = bf16[1,2048,512]{2,1,0:T(8,128)(2,1)} async-done(((bf16[1,512,512]{2,1,0:T(8,128)(2,1)}), bf16[1,2048,512]{2,1,0:T(8,128)(2,1)}) %all-gather.25.cloned.1.call-update) | async-done | bytes 2097168 | tf_op jit(solution)/shard_map/all_gather | solution.py:93
  221.3 5.8 %collective-permute-done.10 = bf16[256,512]{1,0:T(8,128)(2,1)S(1)} collective-permute-done((bf16[256,512]{1,0:T(8,128)(2,1)S(1)}, bf16[256,512]{1,0:T(8,128)(2,1)S(1)}, u32[]{:S(2)}, u32[]{:S(2)}) %collective-permute-start.10) | collective-permute-done | bytes 262176 | tf_op jit(solution)/shard_map/ppermute | solution.py:72
  227.1 5.8 %collective-permute-done.11 = bf16[256,512]{1,0:T(8,128)(2,1)S(1)} collective-permute-done((bf16[256,512]{1,0:T(8,128)(2,1)S(1)}, bf16[256,512]{1,0:T(8,128)(2,1)S(1)}, u32[]{:S(2)}, u32[]{:S(2)}) %collective-permute-start.11) | collective-permute-done | bytes 262176 | tf_op jit(solution)/shard_map/ppermute | solution.py:72
  232.9 5.8 %collective-permute-done.12 = bf16[256,512]{1,0:T(8,128)(2,1)S(1)} collective-permute-done((bf16[256,512]{1,0:T(8,128)(2,1)S(1)}, bf16[256,512]{1,0:T(8,128)(2,1)S(1)}, u32[]{:S(2)}, u32[]{:S(2)}) %collective-permute-start.12) | collective-permute-done | bytes 262176 | tf_op jit(solution)/shard_map/ppermute | solution.py:72
  238.7 2.9 fusion.6
  241.6 5.6 %all-gather.33.cloned.1.call-done = bf16[1,2048,256]{2,1,0:T(8,128)(2,1)} async-done(((bf16[1,512,256]{2,1,0:T(8,128)(2,1)}), bf16[1,2048,256]{2,1,0:T(8,128)(2,1)}) %all-gather.33.cloned.1.call-update) | async-done | bytes 1048592 | tf_op jit(solution)/shard_map/all_gather | solution.py:88
  248.9 3.4 %collective-permute-start.13 = (bf16[8,32,256]{2,1,0:T(8,128)(2,1)S(1)}, bf16[8,32,256]{2,1,0:T(8,128)(2,1)S(1)}, u32[]{:S(2)}, u32[]{:S(2)}) collective-permute-start(bf16[8,32,256]{2,1,0:T(8,128)(2,1)S(1)} %bitcast.107), channel_id=1, source_target_pairs={{0,4},{4,8},{8,12},{1,5},{5,9},{9,13},{2,6},{6,10},{10,14},{3,7},{... | collective-permute-start | bytes 393224 | tf_op jit(solution)/shard_map/ppermute | solution.py:22
  253.6 22.8 %all-gather.35.cloned.1.call-done = bf16[1,256,2048]{1,2,0:T(8,128)(2,1)} async-done(((bf16[1,256,512]{1,2,0:T(8,128)(2,1)}), bf16[1,256,2048]{1,2,0:T(8,128)(2,1)}) %all-gather.35.cloned.1.call-update) | async-done | bytes 1048592 | tf_op jit(solution)/shard_map/all_gather | solution.py:113
  278.6 3.7 %all-to-all-start.2 = ((bf16[256,4,512]{2,0,1:T(8,128)(2,1)}), bf16[256,4,512]{2,0,1:T(8,128)(2,1)S(1)}, u32[]{:S(2)}, u32[]{:S(2)}) async-start(bf16[256,4,512]{2,0,1:T(8,128)(2,1)} %copy.28), calls=%async_computation.2 | async-start | bytes 2097152 | tf_op jit(solution)/shard_map/all_to_all | solution.py:114
  284.3 16.0 %all_gather.46 = bf16[256,1024]{1,0:T(8,128)(2,1)S(1)} all-gather(bf16[256,256]{1,0:T(8,128)(2,1)S(1)} %bitcast.111), channel_id=1, replica_groups=mesh['grp'=2,'sp'=4,'tp'=4] {'tp'}, dimensions={1}, use_global_device_ids=true | all-gather | bytes 655360 | tf_op jit(solution)/shard_map/all_gather | solution.py:112
  300.9 21.9 %all-gather.31.cloned.1.call-done = bf16[1,2048,512]{2,1,0:T(8,128)(2,1)} async-done(((bf16[1,512,512]{2,1,0:T(8,128)(2,1)}), bf16[1,2048,512]{2,1,0:T(8,128)(2,1)}) %all-gather.31.cloned.1.call-update) | async-done | bytes 2097168 | tf_op jit(solution)/shard_map/all_gather | solution.py:93
  322.8 3.1 fusion.69
  (134 shorter events, 33.9 us)
Async XLA Ops:
  6.5 33.1 %all-gather.21.cloned.1.call-start = ((), (), s32[]{:S(2)}) async-start(), calls=%async_computation.4 | async-start | bytes 1310720 | tf_op jit(solution)/shard_map/all_gather | solution.py:88
  8.7 60.1 %all-gather.23.cloned.1.call-start = ((), (), s32[]{:S(2)}) async-start(), calls=%async_computation.5 | async-start | bytes 1310720 | tf_op jit(solution)/shard_map/all_gather | solution.py:113
  9.7 105.5 %all-gather.19.cloned.1.call-start = ((), (), s32[]{:S(2)}) async-start(), calls=%async_computation.3 | async-start | bytes 2621440 | tf_op jit(solution)/shard_map/all_gather | solution.py:93
  11.0 132.5 %all-gather.27.cloned.1.call-start = ((), (), s32[]{:S(2)}) async-start(), calls=%async_computation.7 | async-start | bytes 1310720 | tf_op jit(solution)/shard_map/all_gather | solution.py:88
  11.6 161.2 %all-gather.29.cloned.1.call-start = ((), (), s32[]{:S(2)}) async-start(), calls=%async_computation.8 | async-start | bytes 1310720 | tf_op jit(solution)/shard_map/all_gather | solution.py:113
  12.5 206.3 %all-gather.25.cloned.1.call-start = ((), (), s32[]{:S(2)}) async-start(), calls=%async_computation.6 | async-start | bytes 2621440 | tf_op jit(solution)/shard_map/all_gather | solution.py:93
  12.5 6.5 %collective-permute-start = (bf16[256,512]{1,0:T(8,128)(2,1)S(1)}, bf16[256,512]{1,0:T(8,128)(2,1)S(1)}, u32[]{:S(2)}, u32[]{:S(2)}) collective-permute-start(bf16[256,512]{1,0:T(8,128)(2,1)S(1)} %copy-done.2), channel_id=1, source_target_pairs={{0,1},{1,2},{2,3},{3,0},{4,5},{5,6},{6,7},{7,4},{8,9},{9,10},{10,1... | collective-permute-start | bytes 786440 | tf_op jit(solution)/shard_map/ppermute | solution.py:72
  13.7 57.4 %copy-start.9 = (f32[1,2048]{1,0:T(1,128)}, f32[1,2048]{1,0:T(1,128)S(1)}, u32[]{:S(2)}) copy-start(f32[1,2048]{1,0:T(1,128)S(1)} %get-tuple-element.34) | copy-start | bytes 24580
  19.0 5.8 %collective-permute-start.1 = (bf16[256,512]{1,0:T(8,128)(2,1)S(1)}, bf16[256,512]{1,0:T(8,128)(2,1)S(1)}, u32[]{:S(2)}, u32[]{:S(2)}) collective-permute-start(bf16[256,512]{1,0:T(8,128)(2,1)S(1)} %collective-permute-done), channel_id=1, source_target_pairs={{0,1},{1,2},{2,3},{3,0},{4,5},{5,6},{6,7},{7,4},{8,9},{9,10},{10,1... | collective-permute-start | bytes 786440 | tf_op jit(solution)/shard_map/ppermute | solution.py:72
  24.8 5.8 %collective-permute-start.2 = (bf16[256,512]{1,0:T(8,128)(2,1)S(1)}, bf16[256,512]{1,0:T(8,128)(2,1)S(1)}, u32[]{:S(2)}, u32[]{:S(2)}) collective-permute-start(bf16[256,512]{1,0:T(8,128)(2,1)S(1)} %collective-permute-done.1), channel_id=1, source_target_pairs={{0,1},{1,2},{2,3},{3,0},{4,5},{5,6},{6,7},{7,4},{8,9},{9,10},{10,1... | collective-permute-start | bytes 786440 | tf_op jit(solution)/shard_map/ppermute | solution.py:72
  33.5 37.6 %copy-start.24 = (f32[256]{0:T(256)}, f32[256]{0:T(256)S(1)}, u32[]{:S(2)}) copy-start(f32[256]{0:T(256)S(1)} %add_rsqrt_fusion.2) | copy-start | bytes 3076
  41.4 33.4 %collective-permute-start.3 = (bf16[8,32,256]{2,1,0:T(8,128)(2,1)S(1)}, bf16[8,32,256]{2,1,0:T(8,128)(2,1)S(1)}, u32[]{:S(2)}, u32[]{:S(2)}) collective-permute-start(bf16[8,32,256]{2,1,0:T(8,128)(2,1)S(1)} %bitcast.103), channel_id=1, source_target_pairs={{0,4},{4,8},{8,12},{1,5},{5,9},{9,13},{2,6},{6,10},{10,14},{3,7},{... | collective-permute-start | bytes 393224 | tf_op jit(solution)/shard_map/ppermute | solution.py:22
  44.7 30.0 %collective-permute-start.4 = (bf16[8,32,256]{2,1,0:T(8,128)(2,1)S(1)}, bf16[8,32,256]{2,1,0:T(8,128)(2,1)S(1)}, u32[]{:S(2)}, u32[]{:S(2)}) collective-permute-start(bf16[8,32,256]{2,1,0:T(8,128)(2,1)S(1)} %bitcast.104), channel_id=1, source_target_pairs={{4,0},{8,4},{12,8},{5,1},{9,5},{13,9},{6,2},{10,6},{14,10},{7,3},{... | collective-permute-start | bytes 393224 | tf_op jit(solution)/shard_map/ppermute | solution.py:23
  71.1 21.8 %all-to-all-start = ((bf16[256,4,512]{2,0,1:T(8,128)(2,1)}), bf16[256,4,512]{2,0,1:T(8,128)(2,1)S(1)}, u32[]{:S(2)}, u32[]{:S(2)}) async-start(bf16[256,4,512]{2,0,1:T(8,128)(2,1)} %copy.20), calls=%async_computation | async-start | bytes 2097152 | tf_op jit(solution)/shard_map/all_to_all | solution.py:114
  74.7 172.5 %all-gather.33.cloned.1.call-start = ((), (), s32[]{:S(2)}) async-start(), calls=%async_computation.10 | async-start | bytes 1310720 | tf_op jit(solution)/shard_map/all_gather | solution.py:88
  117.7 5.8 %collective-permute-start.5 = (bf16[256,512]{1,0:T(8,128)(2,1)S(1)}, bf16[256,512]{1,0:T(8,128)(2,1)S(1)}, u32[]{:S(2)}, u32[]{:S(2)}) collective-permute-start(bf16[256,512]{1,0:T(8,128)(2,1)S(1)} %fusion.75), channel_id=1, source_target_pairs={{0,1},{1,2},{2,3},{3,0},{4,5},{5,6},{6,7},{7,4},{8,9},{9,10},{10,1... | collective-permute-start | bytes 786440 | tf_op jit(solution)/shard_map/ppermute | solution.py:72
  117.8 158.5 %all-gather.35.cloned.1.call-start = ((), (), s32[]{:S(2)}) async-start(), calls=%async_computation.11 | async-start | bytes 1310720 | tf_op jit(solution)/shard_map/all_gather | solution.py:113
  123.6 5.8 %collective-permute-start.6 = (bf16[256,512]{1,0:T(8,128)(2,1)S(1)}, bf16[256,512]{1,0:T(8,128)(2,1)S(1)}, u32[]{:S(2)}, u32[]{:S(2)}) collective-permute-start(bf16[256,512]{1,0:T(8,128)(2,1)S(1)} %collective-permute-done.5), channel_id=1, source_target_pairs={{0,1},{1,2},{2,3},{3,0},{4,5},{5,6},{6,7},{7,4},{8,9},{9,10},{10,1... | collective-permute-start | bytes 786440 | tf_op jit(solution)/shard_map/ppermute | solution.py:72
  129.4 5.8 %collective-permute-start.7 = (bf16[256,512]{1,0:T(8,128)(2,1)S(1)}, bf16[256,512]{1,0:T(8,128)(2,1)S(1)}, u32[]{:S(2)}, u32[]{:S(2)}) collective-permute-start(bf16[256,512]{1,0:T(8,128)(2,1)S(1)} %collective-permute-done.6), channel_id=1, source_target_pairs={{0,1},{1,2},{2,3},{3,0},{4,5},{5,6},{6,7},{7,4},{8,9},{9,10},{10,1... | collective-permute-start | bytes 786440 | tf_op jit(solution)/shard_map/ppermute | solution.py:72
  138.0 37.0 %copy-start.22 = (f32[256]{0:T(256)}, f32[256]{0:T(256)S(1)}, u32[]{:S(2)}) copy-start(f32[256]{0:T(256)S(1)} %add_rsqrt_fusion.1) | copy-start | bytes 3076
  145.2 33.4 %collective-permute-start.8 = (bf16[8,32,256]{2,1,0:T(8,128)(2,1)S(1)}, bf16[8,32,256]{2,1,0:T(8,128)(2,1)S(1)}, u32[]{:S(2)}, u32[]{:S(2)}) collective-permute-start(bf16[8,32,256]{2,1,0:T(8,128)(2,1)S(1)} %bitcast.99), channel_id=1, source_target_pairs={{0,4},{4,8},{8,12},{1,5},{5,9},{9,13},{2,6},{6,10},{10,14},{3,7},{... | collective-permute-start | bytes 393224 | tf_op jit(solution)/shard_map/ppermute | solution.py:22
  148.6 30.1 %collective-permute-start.9 = (bf16[8,32,256]{2,1,0:T(8,128)(2,1)S(1)}, bf16[8,32,256]{2,1,0:T(8,128)(2,1)S(1)}, u32[]{:S(2)}, u32[]{:S(2)}) collective-permute-start(bf16[8,32,256]{2,1,0:T(8,128)(2,1)S(1)} %bitcast.100), channel_id=1, source_target_pairs={{4,0},{8,4},{12,8},{5,1},{9,5},{13,9},{6,2},{10,6},{14,10},{7,3},{... | collective-permute-start | bytes 393224 | tf_op jit(solution)/shard_map/ppermute | solution.py:23
  175.1 21.8 %all-to-all-start.1 = ((bf16[256,4,512]{2,0,1:T(8,128)(2,1)}), bf16[256,4,512]{2,0,1:T(8,128)(2,1)S(1)}, u32[]{:S(2)}, u32[]{:S(2)}) async-start(bf16[256,4,512]{2,0,1:T(8,128)(2,1)} %copy.24), calls=%async_computation.1 | async-start | bytes 2097152 | tf_op jit(solution)/shard_map/all_to_all | solution.py:114
  178.6 144.2 %all-gather.31.cloned.1.call-start = ((), (), s32[]{:S(2)}) async-start(), calls=%async_computation.9 | async-start | bytes 2621440 | tf_op jit(solution)/shard_map/all_gather | solution.py:93
  180.5 38.2 %copy-start.8 = (f32[1,2048]{1,0:T(1,128)S(1)}, f32[1,2048]{1,0:T(1,128)}, u32[]{:S(2)}) copy-start(f32[1,2048]{1,0:T(1,128)} %get-tuple-element.35) | copy-start | bytes 24580
  180.6 38.2 %copy-start.23 = (f32[256]{0:T(256)S(1)}, f32[256]{0:T(256)}, u32[]{:S(2)}) copy-start(f32[256]{0:T(256)} %copy-done.22) | copy-start | bytes 3076
  221.2 5.8 %collective-permute-start.10 = (bf16[256,512]{1,0:T(8,128)(2,1)S(1)}, bf16[256,512]{1,0:T(8,128)(2,1)S(1)}, u32[]{:S(2)}, u32[]{:S(2)}) collective-permute-start(bf16[256,512]{1,0:T(8,128)(2,1)S(1)} %fusion.72), channel_id=1, source_target_pairs={{0,1},{1,2},{2,3},{3,0},{4,5},{5,6},{6,7},{7,4},{8,9},{9,10},{10,1... | collective-permute-start | bytes 786440 | tf_op jit(solution)/shard_map/ppermute | solution.py:72
  227.1 5.8 %collective-permute-start.11 = (bf16[256,512]{1,0:T(8,128)(2,1)S(1)}, bf16[256,512]{1,0:T(8,128)(2,1)S(1)}, u32[]{:S(2)}, u32[]{:S(2)}) collective-permute-start(bf16[256,512]{1,0:T(8,128)(2,1)S(1)} %collective-permute-done.10), channel_id=1, source_target_pairs={{0,1},{1,2},{2,3},{3,0},{4,5},{5,6},{6,7},{7,4},{8,9},{9,10},{10,1... | collective-permute-start | bytes 786440 | tf_op jit(solution)/shard_map/ppermute | solution.py:72
  232.9 5.8 %collective-permute-start.12 = (bf16[256,512]{1,0:T(8,128)(2,1)S(1)}, bf16[256,512]{1,0:T(8,128)(2,1)S(1)}, u32[]{:S(2)}, u32[]{:S(2)}) collective-permute-start(bf16[256,512]{1,0:T(8,128)(2,1)S(1)} %collective-permute-done.11), channel_id=1, source_target_pairs={{0,1},{1,2},{2,3},{3,0},{4,5},{5,6},{6,7},{7,4},{8,9},{9,10},{10,1... | collective-permute-start | bytes 786440 | tf_op jit(solution)/shard_map/ppermute | solution.py:72
  248.9 33.5 %collective-permute-start.13 = (bf16[8,32,256]{2,1,0:T(8,128)(2,1)S(1)}, bf16[8,32,256]{2,1,0:T(8,128)(2,1)S(1)}, u32[]{:S(2)}, u32[]{:S(2)}) collective-permute-start(bf16[8,32,256]{2,1,0:T(8,128)(2,1)S(1)} %bitcast.107), channel_id=1, source_target_pairs={{0,4},{4,8},{8,12},{1,5},{5,9},{9,13},{2,6},{6,10},{10,14},{3,7},{... | collective-permute-start | bytes 393224 | tf_op jit(solution)/shard_map/ppermute | solution.py:22
  252.3 30.1 %collective-permute-start.14 = (bf16[8,32,256]{2,1,0:T(8,128)(2,1)S(1)}, bf16[8,32,256]{2,1,0:T(8,128)(2,1)S(1)}, u32[]{:S(2)}, u32[]{:S(2)}) collective-permute-start(bf16[8,32,256]{2,1,0:T(8,128)(2,1)S(1)} %bitcast.108), channel_id=1, source_target_pairs={{4,0},{8,4},{12,8},{5,1},{9,5},{13,9},{6,2},{10,6},{14,10},{7,3},{... | collective-permute-start | bytes 393224 | tf_op jit(solution)/shard_map/ppermute | solution.py:23
  278.6 21.8 %all-to-all-start.2 = ((bf16[256,4,512]{2,0,1:T(8,128)(2,1)}), bf16[256,4,512]{2,0,1:T(8,128)(2,1)S(1)}, u32[]{:S(2)}, u32[]{:S(2)}) async-start(bf16[256,4,512]{2,0,1:T(8,128)(2,1)} %copy.28), calls=%async_computation.2 | async-start | bytes 2097152 | tf_op jit(solution)/shard_map/all_to_all | solution.py:114
  (20 other events, 237.1 us)
Sparse Core Ops, SparseCore 0:
  8.9 30.6 all-gather.20
  41.2 27.5 all-gather.22
  70.4 44.8 all-gather.18
  116.7 26.7 all-gather.26
  144.9 27.8 all-gather.28
  174.2 44.5 all-gather.24
  220.4 26.7 all-gather.32
  248.7 27.5 all-gather.34
  277.9 44.8 all-gather.30
